TPU v7x, 32 devices: a whole 2x2x4 slice. The times are simulated.
32 devices in a mesh: fs: 8 (over z, y), tp: 4 (over x, core).
Axes of the slice: x: 2, y: 2, z: 4, core: 2. Of those that a mesh axis runs over, the one named last changes fastest.
Arguments:
- inputs: bfloat16 [6144, 2048], P('fs'), may hold values from -6 to 6
- values_cot: bfloat16 [6144, 2048], P('fs', 'tp'), may hold values from -0.22949219 to 0.22949219
- decay_cot: bfloat16 [6144, 16], P('fs'), may hold values from -0.22949219 to 0.22949219
- factor: bfloat16 [2048, 512], P('fs', 'tp'), may hold values from -0.125 to 0.125
- value_weight: float32 [2048, 2048], P('fs', 'tp'), may hold values from -3 to 3
- lowrank_mean: float32 [512, 2048], P('fs', 'tp'), may hold values from -60 to 60
- lowrank_var: float32 [512, 2048], P('fs', 'tp'), may hold values from 0.3 to 3
- decay_weight: float32 [2048, 16], replicated, may hold values from -3 to 3
- decay_mean: float32 [2048, 16], replicated, may hold values from -6 to 6
- decay_var: float32 [2048, 16], replicated, may hold values from 0.3 to 3
Outputs:
- value_step: float32 [2048, 2048], P('fs', 'tp')
- value_new: float32 [2048, 2048], P('fs', 'tp')
- value_copy: bfloat16 [2048, 2048], P('fs', 'tp')
- mean_new: float32 [512, 2048], P('fs', 'tp')
- var_new: float32 [512, 2048], P('fs', 'tp')
- decay_new: float32 [2048, 16], replicated
- decay_copy: bfloat16 [2048, 16], replicated
- decay_mean_new: float32 [2048, 16], replicated
- decay_var_new: float32 [2048, 16], replicated
All inputs are finite; a program needn't handle non-finite values.
Results may differ from a plain program's by a relative error of at most 0.0042.
Values may be sent and summed in bfloat16 or wider, within the bound.
A program may use at most 64 MiB of HBM per device.

v0:
```python
import jax
import jax.numpy as jnp
from jax import lax
from jax.sharding import PartitionSpec as P

W = 2048
R = 512


def local(
    inputs,
    values_cot,
    decay_cot,
    factor,
    value_weight,
    lowrank_mean,
    lowrank_var,
    decay_weight,
    decay_mean,
    decay_var,
):
    own_rows = lax.all_gather(factor, "tp", axis=1, tiled=True)
    quarter = jnp.dot(
        inputs, lax.all_gather(factor, "fs", axis=0, tiled=True), preferred_element_type=jnp.float32
    ).astype(jnp.bfloat16)
    projected = lax.all_gather(quarter, "tp", axis=1, tiled=True)
    lowrank_grad = lax.psum_scatter(
        lax.dot_general(
            projected, values_cot, (((0,), (0,)), ((), ())), preferred_element_type=jnp.float32
        ),
        "fs",
        scatter_dimension=0,
        tiled=True,
    )
    mean_new = 0.9 * lowrank_mean + 0.1 * lowrank_grad
    var_new = 0.95 * lowrank_var + 0.05 * lowrank_grad * lowrank_grad
    adam_ratio = mean_new / (jnp.sqrt(var_new) + 1e-08)
    full_ratio = lax.all_gather(adam_ratio, "fs", axis=0, tiled=True)
    squares = lax.psum(jnp.sum(adam_ratio * adam_ratio), ("fs", "tp"))
    root_mean = jnp.sqrt(squares / (R * W) + 1e-06)
    delta = jnp.dot(own_rows.astype(jnp.float32), full_ratio, precision=lax.Precision.HIGHEST)
    value_step = -0.5 / root_mean * delta
    value_new = value_weight + value_step
    value_copy = value_new.astype(jnp.bfloat16)
    decay_part = lax.dot_general(
        inputs, decay_cot, (((0,), (0,)), ((), ())), preferred_element_type=jnp.float32
    )
    decay_grad = lax.psum(decay_part, "fs")
    decay_mean_new = 0.9 * decay_mean + 0.1 * decay_grad
    decay_var_new = 0.95 * decay_var + 0.05 * decay_grad * decay_grad
    decay_new = decay_weight - 0.5 * decay_mean_new / (jnp.sqrt(decay_var_new) + 1e-08)
    decay_copy = decay_new.astype(jnp.bfloat16)
    return (
        value_step,
        value_new,
        value_copy,
        mean_new,
        var_new,
        decay_new,
        decay_copy,
        decay_mean_new,
        decay_var_new,
    )


def solution(mesh):
    in_specs = (
        P("fs", None),
        P("fs", "tp"),
        P("fs", None),
        P("fs", "tp"),
        P("fs", "tp"),
        P("fs", "tp"),
        P("fs", "tp"),
        P(),
        P(),
        P(),
    )
    out_specs = (
        P("fs", "tp"),
        P("fs", "tp"),
        P("fs", "tp"),
        P("fs", "tp"),
        P("fs", "tp"),
        P(),
        P(),
        P(),
        P(),
    )
    return jax.shard_map(local, mesh=mesh, in_specs=in_specs, out_specs=out_specs, check_vma=False)
```

profile of v0, /device:TPU:0, one launch (start us, length us, event | category | flops | bytes accessed | tf_op | source)
XLA Modules:
  0.0 248.1 jit_solution(9775094986767670953)
XLA Ops:
  7.2 0.0 copy-start
  7.2 0.0 reduce-scatter.2.cloned.1.call-start
  7.2 33.4 %all_gather.12 = bf16[2048,128]{1,0:T(8,128)(2,1)S(1)} all-gather(bf16[256,128]{1,0:T(8,128)(2,1)} %param.13), channel_id=1, replica_groups=mesh['fs'=8,'tp'=4] {'fs'}, dimensions={0}, use_global_device_ids=true | all-gather | bytes 589824 | tf_op jit(solution)/shard_map/all_gather | solution.py:24
  40.6 1.0 convolution_convert_fusion
  41.6 8.6 %all_gather.13 = bf16[768,512]{1,0:T(8,128)(2,1)S(1)} all-gather(bf16[768,128]{1,0:T(8,128)(2,1)S(1)} %convolution_convert_fusion), channel_id=1, replica_groups=mesh['fs'=8,'tp'=4] {'tp'}, dimensions={1}, use_global_device_ids=true | all-gather | bytes 983040 | tf_op jit(solution)/shard_map/all_gather | solution.py:26
  50.2 1.6 fusion.7
  51.8 0.0 reduce-scatter.2.cloned.1.call-update
  51.8 0.0 all-reduce.2.cloned.1.call-start
  51.9 1.2 fusion.8
  53.1 0.0 all-reduce.2.cloned.1.call-update
  53.1 0.0 all-gather.2.cloned.1.call-start
  53.2 63.2 %reduce-scatter.2.cloned.1.call-done = f32[64,512]{1,0:T(8,128)} async-done(((f32[512,512]{1,0:T(8,128)}), f32[64,512]{1,0:T(8,128)}) %reduce-scatter.2.cloned.1.call-update) | async-done | bytes 131088 | tf_op jit(solution)/shard_map/reduce_scatter | solution.py:27
  116.3 2.3 multiply_reduce_fusion
  118.6 0.0 all-gather.2.cloned.1.call-update
  118.6 2.0 copy.19
  120.7 5.8 %all_gather.15 = bf16[256,512]{1,0:T(8,128)(2,1)S(1)} all-gather(bf16[256,128]{1,0:T(8,128)(2,1)S(1)} %copy-done.2), channel_id=1, replica_groups=mesh['fs'=8,'tp'=4] {'tp'}, dimensions={1}, use_global_device_ids=true | all-gather | bytes 327680 | tf_op jit(solution)/shard_map/all_gather | solution.py:22
  126.5 63.3 %all-reduce.2.cloned.1.call-done = f32[2048,16]{0,1:T(8,128)} async-done(((f32[2048,16]{0,1:T(8,128)}), f32[2048,16]{0,1:T(8,128)}) %all-reduce.2.cloned.1.call-update) | async-done | bytes 131088 | tf_op jit(solution)/shard_map/psum | solution.py:48
  189.7 1.9 fusion.3
  191.6 39.9 %psum.14 = f32[]{:T(128)} all-reduce(f32[]{:T(128)} %get-tuple-element.24), channel_id=1, replica_groups=mesh['fs'=8,'tp'=4] {'fs','tp'}, use_global_device_ids=true, to_apply=%region_2.0 | all-reduce | flops 1 | bytes 8 | tf_op jit(solution)/shard_map/psum | solution.py:39
  232.3 0.0 all-gather.2.cloned.1.call-done
  232.3 3.4 %fusion.5 = (bf16[256,512]{0,1:T(8,128)(2,1)}, f32[256,512]{0,1:T(8,128)}, f32[256,512]{0,1:T(8,128)}) fusion(f32[256,512]{0,1:T(8,128)} %copy.19, f32[512,512]{1,0:T(8,128)} %all-gather.2.cloned.1.call-done, bf16[256,512]{1,0:T(8,128)(2,1)S(1)} %all_gather.15, f32[]{:T(128)S(6)} %div.14), kind=kOutput, calls=%fused_computation.13 | convolution fusion | flops 805699584 | bytes 3145732 | tf_op jit(solution)/shard_map/dot_general | solution.py:41
  235.7 2.0 copy.20
  237.7 2.0 copy.21
  239.8 1.8 copy.22
  (11 shorter events, 0.0 us)
Async XLA Ops:
  7.2 33.4 %copy-start = (bf16[768,2048]{1,0:T(8,128)(2,1)S(1)}, bf16[768,2048]{1,0:T(8,128)(2,1)}, u32[]{:S(2)}) copy-start(bf16[768,2048]{1,0:T(8,128)(2,1)} %param.10) | copy-start | bytes 9437188
  7.2 109.1 %reduce-scatter.2.cloned.1.call-start = ((), (), s32[]{:S(2)}) async-start(), calls=%async_computation.1 | async-start | bytes 1179648 | tf_op jit(solution)/shard_map/reduce_scatter | solution.py:27
  40.6 9.6 %copy-start.1 = (bf16[768,512]{1,0:T(8,128)(2,1)S(1)}, bf16[768,512]{1,0:T(8,128)(2,1)}, u32[]{:S(2)}) copy-start(bf16[768,512]{1,0:T(8,128)(2,1)} %param.11) | copy-start | bytes 2359300
  41.6 10.3 %copy-start.5 = (bf16[768,16]{0,1:T(8,128)(2,1)S(1)}, bf16[768,16]{0,1:T(8,128)(2,1)}, u32[]{:S(2)}) copy-start(bf16[768,16]{0,1:T(8,128)(2,1)} %param.12) | copy-start | bytes 73732
  50.2 66.1 %copy-start.3 = (f32[64,512]{1,0:T(8,128)S(1)}, f32[64,512]{1,0:T(8,128)}, u32[]{:S(2)}) copy-start(f32[64,512]{1,0:T(8,128)} %param.16) | copy-start | bytes 393220
  50.2 66.1 %copy-start.4 = (f32[64,512]{1,0:T(8,128)S(1)}, f32[64,512]{1,0:T(8,128)}, u32[]{:S(2)}) copy-start(f32[64,512]{1,0:T(8,128)} %param.15) | copy-start | bytes 393220
  51.8 68.9 %copy-start.2 = (bf16[256,128]{1,0:T(8,128)(2,1)S(1)}, bf16[256,128]{1,0:T(8,128)(2,1)}, u32[]{:S(2)}) copy-start(bf16[256,128]{1,0:T(8,128)(2,1)} %param.13) | copy-start | bytes 196612
  51.8 137.9 %all-reduce.2.cloned.1.call-start = ((), (), s32[]{:S(2)}) async-start(), calls=%async_computation.3 | async-start | bytes 262144 | tf_op jit(solution)/shard_map/psum | solution.py:48
  53.1 179.2 %all-gather.2.cloned.1.call-start = ((), (), s32[]{:S(2)}) async-start(), calls=%async_computation.2 | async-start | bytes 1179648 | tf_op jit(solution)/shard_map/all_gather | solution.py:38
Sparse Core Ops, SparseCore 0:
  52.0 64.3 reduce-scatter.1
  120.3 69.4 all-reduce.1
  192.4 39.6 all-gather.1
where the time goes:
time: 249 us; the launch traced here: 248 us
  waiting for transfers between devices  127 us (51%)
  blocking collectives  87.7 us (35%)
  between operations  14.5 us (6%)
  local copies, waits for them, and re-layouts  7.93 us (3%)
  matrix products  7.14 us (3%)
  other arithmetic  4.16 us (2%)
    psum x1, waiting for transfers between devices, local(): decay_grad = lax.psum(decay_part, 'fs')  63.3 us
    reduce_scatter x1, waiting for transfers between devices, local(): lax.psum_scatter(lax.dot_general(projected, values_cot, (((0,), (0,)), ((...  63.2 us
    psum x1, blocking collectives, local(): squares = lax.psum(jnp.sum(adam_ratio * adam_ratio), ('fs', 'tp'))  39.9 us
    all_gather x1, blocking collectives, local(): lax.all_gather(factor, 'fs', axis=0, tiled=True)  33.4 us
    all_gather x1, blocking collectives, local(): projected = lax.all_gather(quarter, 'tp', axis=1, tiled=True)  8.62 us
    unnamed x16, local copies, waits for them, and re-layouts  7.93 us
    all_gather x1, blocking collectives, local(): own_rows = lax.all_gather(factor, 'tp', axis=1, tiled=True)  5.79 us
  transfers between devices with their start and end apart: 3, of which 2 were waited for; matrix products, arithmetic and copies ran while one was open for 3% of the time, Pallas kernels for 0%

commit v1 on v0

--- a/solution.py
+++ b/solution.py
@@ -45,7 +45,7 @@
     decay_part = lax.dot_general(
         inputs, decay_cot, (((0,), (0,)), ((), ())), preferred_element_type=jnp.float32
     )
-    decay_grad = lax.psum(decay_part, "fs")
+    decay_grad = jnp.sum(lax.all_gather(decay_part, "fs"), axis=0)
     decay_mean_new = 0.9 * decay_mean + 0.1 * decay_grad
     decay_var_new = 0.95 * decay_var + 0.05 * decay_grad * decay_grad
     decay_new = decay_weight - 0.5 * decay_mean_new / (jnp.sqrt(decay_var_new) + 1e-08)

time: 249 us -> 218 us (0.88)
  waiting for transfers between devices: 127 us -> 95.2 us
    psum x1 -> x0, waiting for transfers between devices: 63.3 us -> none  [local(): decay_grad = lax.psum(decay_part, 'fs')]
    all_gather x0 -> x1, waiting for transfers between devices: none -> 31.9 us  [local(): decay_grad = jnp.sum(lax.all_gather(decay_part, 'fs'), axis=0)]
    unnamed x16 -> x17, local copies, waits for them, and re-layouts: 7.93 us -> 9.77 us
  transfers between devices with their start and end apart: 3 -> 3, of which waited for: 2 -> 2; matrix products, arithmetic and copies ran while one was open for 3% -> 4% of each run, Pallas kernels for 0% -> 0%
where the time goes in v1:
time: 218 us; the launch traced here: 217 us
  waiting for transfers between devices  95.2 us (44%)
  blocking collectives  86.2 us (40%)
  between operations  14.5 us (7%)
  local copies, waits for them, and re-layouts  9.77 us (4%)
  matrix products  7.13 us (3%)
  other arithmetic  4.36 us (2%)
    reduce_scatter x1, waiting for transfers between devices, local(): lax.psum_scatter(lax.dot_general(projected, values_cot, (((0,), (0,)), ((...  63.2 us
    psum x1, blocking collectives, local(): squares = lax.psum(jnp.sum(adam_ratio * adam_ratio), ('fs', 'tp'))  38.4 us
    all_gather x1, blocking collectives, local(): lax.all_gather(factor, 'fs', axis=0, tiled=True)  33.4 us
    all_gather x1, waiting for transfers between devices, local(): decay_grad = jnp.sum(lax.all_gather(decay_part, 'fs'), axis=0)  31.9 us
    unnamed x17, local copies, waits for them, and re-layouts  9.77 us
    all_gather x1, blocking collectives, local(): projected = lax.all_gather(quarter, 'tp', axis=1, tiled=True)  8.62 us
    all_gather x1, blocking collectives, local(): own_rows = lax.all_gather(factor, 'tp', axis=1, tiled=True)  5.79 us
  transfers between devices with their start and end apart: 3, of which 2 were waited for; matrix products, arithmetic and copies ran while one was open for 4% of the time, Pallas kernels for 0%

profile of v1, /device:TPU:0, one launch (start us, length us, event | category | flops | bytes accessed | tf_op | source)
XLA Modules:
  0.0 217.2 jit_solution(13201608651313082040)
XLA Ops:
  7.2 0.0 reduce-scatter.2.cloned.1.call-start
  7.2 33.4 %all_gather.18 = bf16[2048,128]{1,0:T(8,128)(2,1)S(1)} all-gather(bf16[256,128]{1,0:T(8,128)(2,1)} %param.13), channel_id=1, replica_groups=mesh['fs'=8,'tp'=4] {'fs'}, dimensions={0}, use_global_device_ids=true | all-gather | bytes 589824 | tf_op jit(solution)/shard_map/all_gather | solution.py:24
  40.6 1.0 convolution_convert_fusion
  41.6 8.6 %all_gather.19 = bf16[768,512]{1,0:T(8,128)(2,1)S(1)} all-gather(bf16[768,128]{1,0:T(8,128)(2,1)S(1)} %convolution_convert_fusion), channel_id=1, replica_groups=mesh['fs'=8,'tp'=4] {'tp'}, dimensions={1}, use_global_device_ids=true | all-gather | bytes 983040 | tf_op jit(solution)/shard_map/all_gather | solution.py:26
  50.2 1.6 fusion.7
  51.8 0.0 reduce-scatter.2.cloned.1.call-update
  51.8 0.0 all-gather.6.cloned.1.call-start
  51.9 1.2 fusion.8
  53.1 0.0 all-gather.4.cloned.1.call-start
  53.2 63.2 %reduce-scatter.2.cloned.1.call-done = f32[64,512]{1,0:T(8,128)} async-done(((f32[512,512]{1,0:T(8,128)}), f32[64,512]{1,0:T(8,128)}) %reduce-scatter.2.cloned.1.call-update) | async-done | bytes 131088 | tf_op jit(solution)/shard_map/reduce_scatter | solution.py:27
  116.3 2.3 %multiply_reduce_fusion = (f32[]{:T(128)}, f32[64,512]{1,0:T(8,128)}, f32[64,512]{1,0:T(8,128)}, f32[64,512]{1,0:T(8,128)}) fusion(f32[64,512]{1,0:T(8,128)} %reduce-scatter.2.cloned.1.call-done, f32[64,512]{1,0:T(8,128)S(1)} %copy-done.3, f32[64,512]{1,0:T(8,128)S(1)} %copy-done.4), kind=kLoop, calls=%fused_computation.10 | loop fusion | flops 360447 | bytes 786436 | tf_op jit(solution)/shard_map/reduce_sum | solution.py:39
  118.6 0.0 all-gather.4.cloned.1.call-update
  118.6 2.0 copy.19
  120.7 5.8 %all_gather.21 = bf16[256,512]{1,0:T(8,128)(2,1)S(1)} all-gather(bf16[256,128]{1,0:T(8,128)(2,1)S(1)} %copy-done.2), channel_id=1, replica_groups=mesh['fs'=8,'tp'=4] {'tp'}, dimensions={1}, use_global_device_ids=true | all-gather | bytes 327680 | tf_op jit(solution)/shard_map/all_gather | solution.py:22
  126.5 31.9 %all-gather.6.cloned.1.call-done = f32[16384,16]{0,1:T(8,128)} async-done(((f32[2048,16]{0,1:T(8,128)}), f32[16384,16]{0,1:T(8,128)}) %all-gather.6.cloned.1.call-update) | async-done | bytes 1048592 | tf_op jit(solution)/shard_map/all_gather | solution.py:48
  158.4 1.8 copy.23
  160.2 0.3 bitcast_reduce_fusion
  160.5 1.8 fusion.3
  162.3 38.4 %psum.7 = f32[]{:T(128)} all-reduce(f32[]{:T(128)} %get-tuple-element.24), channel_id=1, replica_groups=mesh['fs'=8,'tp'=4] {'fs','tp'}, use_global_device_ids=true, to_apply=%region_2.0 | all-reduce | flops 1 | bytes 8 | tf_op jit(solution)/shard_map/psum | solution.py:39
  201.4 0.0 all-gather.4.cloned.1.call-done
  201.4 3.4 %fusion.5 = (bf16[256,512]{0,1:T(8,128)(2,1)}, f32[256,512]{0,1:T(8,128)}, f32[256,512]{0,1:T(8,128)}) fusion(f32[256,512]{0,1:T(8,128)} %copy.19, f32[512,512]{1,0:T(8,128)} %all-gather.4.cloned.1.call-done, bf16[256,512]{1,0:T(8,128)(2,1)S(1)} %all_gather.21, f32[]{:T(128)S(6)} %div.14), kind=kOutput, calls=%fused_computation.14 | convolution fusion | flops 805699584 | bytes 3145732 | tf_op jit(solution)/shard_map/dot_general | solution.py:41
  204.8 1.8 copy.22
  206.6 2.0 copy.21
  208.7 2.0 copy.20
  (13 shorter events, 0.0 us)
Async XLA Ops:
  7.2 33.4 %copy-start = (bf16[768,2048]{1,0:T(8,128)(2,1)S(1)}, bf16[768,2048]{1,0:T(8,128)(2,1)}, u32[]{:S(2)}) copy-start(bf16[768,2048]{1,0:T(8,128)(2,1)} %param.10) | copy-start | bytes 9437188
  7.2 109.1 %reduce-scatter.2.cloned.1.call-start = ((), (), s32[]{:S(2)}) async-start(), calls=%async_computation.1 | async-start | bytes 1179648 | tf_op jit(solution)/shard_map/reduce_scatter | solution.py:27
  40.6 9.6 %copy-start.1 = (bf16[768,512]{1,0:T(8,128)(2,1)S(1)}, bf16[768,512]{1,0:T(8,128)(2,1)}, u32[]{:S(2)}) copy-start(bf16[768,512]{1,0:T(8,128)(2,1)} %param.11) | copy-start | bytes 2359300
  41.6 10.3 %copy-start.5 = (bf16[768,16]{0,1:T(8,128)(2,1)S(1)}, bf16[768,16]{0,1:T(8,128)(2,1)}, u32[]{:S(2)}) copy-start(bf16[768,16]{0,1:T(8,128)(2,1)} %param.12) | copy-start | bytes 73732
  50.2 66.1 %copy-start.3 = (f32[64,512]{1,0:T(8,128)S(1)}, f32[64,512]{1,0:T(8,128)}, u32[]{:S(2)}) copy-start(f32[64,512]{1,0:T(8,128)} %param.16) | copy-start | bytes 393220
  50.2 66.1 %copy-start.4 = (f32[64,512]{1,0:T(8,128)S(1)}, f32[64,512]{1,0:T(8,128)}, u32[]{:S(2)}) copy-start(f32[64,512]{1,0:T(8,128)} %param.15) | copy-start | bytes 393220
  51.8 68.9 %copy-start.2 = (bf16[256,128]{1,0:T(8,128)(2,1)S(1)}, bf16[256,128]{1,0:T(8,128)(2,1)}, u32[]{:S(2)}) copy-start(bf16[256,128]{1,0:T(8,128)(2,1)} %param.13) | copy-start | bytes 196612
  51.8 106.6 %all-gather.6.cloned.1.call-start = ((), (), s32[]{:S(2)}) async-start(), calls=%async_computation.3 | async-start | bytes 1179648 | tf_op jit(solution)/shard_map/all_gather | solution.py:48
  53.1 148.3 %all-gather.4.cloned.1.call-start = ((), (), s32[]{:S(2)}) async-start(), calls=%async_computation.2 | async-start | bytes 1179648 | tf_op jit(solution)/shard_map/all_gather | solution.py:38
Sparse Core Ops, SparseCore 0:
  52.0 64.3 reduce-scatter.1
  119.1 39.2 all-gather.5
  161.1 39.0 all-gather.3
